TPU v7x, 256 devices: a 8x8x2 block of a 8x8x16 slice. The times are simulated.
256 devices in a mesh: grp: 2 (over z), fs: 16 (over y, core), tp: 8 (over x).
Axes of the slice: x: 8, y: 8, z: 2, core: 2. Of those that a mesh axis runs over, the one named last changes fastest.
The devices are a block of a 8x8x16 slice.
Arguments:
- stream: bfloat16 [32768, 2048], P(('grp', 'fs', 'tp')), parts along dimension 0, may hold values from -4 to 4
- gain_first: bfloat16 [2048], replicated, may hold values from 0.099609375 to 1.8984375
- gate_first: bfloat16 [2048, 4096], P('fs', 'tp'), may hold values from -0.125 to 0.125
- up_first: bfloat16 [2048, 4096], P('fs', 'tp'), may hold values from -0.125 to 0.125
- down_first: bfloat16 [4096, 2048], P('tp', 'fs'), may hold values from -0.09375 to 0.09375
- gain_second: bfloat16 [2048], replicated, may hold values from 0.099609375 to 1.8984375
- gate_second: bfloat16 [2048, 4096], P('fs', 'tp'), may hold values from -0.125 to 0.125
- up_second: bfloat16 [2048, 4096], P('fs', 'tp'), may hold values from -0.125 to 0.125
- down_second: bfloat16 [4096, 2048], P('tp', 'fs'), may hold values from -0.09375 to 0.09375
Outputs:
- result: bfloat16 [32768, 2048], P(('grp', 'fs', 'tp')), parts along dimension 0
There are 2 independent parts, one for each index of `grp`. A program takes and returns all parts, laid end to end along the dimension named above; an argument that names none is the same for every part. Nothing has to cross between parts.
All inputs are finite; a program needn't handle non-finite values.
Results may differ from a plain program's by a relative error of at most 0.018.
Values may be sent and summed in bfloat16 or wider, within the bound.
A program may use at most 64 MiB of HBM per device.

v0:
```python
import jax
import jax.numpy as jnp
from jax import lax
from jax.sharding import PartitionSpec as P


def gather_turned(arrays, axis, dims):
    turned = [jnp.moveaxis(a, dim, 0) for a, dim in zip(arrays, dims)]
    widths = [t[0].size for t in turned]
    both = jnp.concatenate([t.reshape(-1, w) for t, w in zip(turned, widths)], axis=1)
    result = lax.all_gather(both, axis, axis=0, tiled=True)
    blocks = jnp.split(result, [sum(widths[:k]) for k in range(1, len(widths))], axis=1)
    return tuple(
        (
            jnp.moveaxis(b.reshape(-1, *t.shape[1:]), 0, dim)
            for b, t, dim in zip(blocks, turned, dims)
        )
    )


def half_branch(stream, gain, gathered):
    stream_f = stream.astype(jnp.float32)
    normed = (
        stream_f
        * lax.rsqrt(jnp.mean(stream_f * stream_f, axis=-1, keepdims=True) + 1e-06)
        * gain.astype(jnp.float32)
    ).astype(jnp.bfloat16)
    tokens = lax.all_gather(normed, "tp", axis=0, tiled=True)
    gate_act = jnp.dot(tokens, gathered[0], preferred_element_type=jnp.float32)
    up_act = jnp.dot(tokens, gathered[1], preferred_element_type=jnp.float32)
    down_full = gathered[2]
    hidden = (jax.nn.silu(gate_act) * up_act).astype(jnp.bfloat16)
    summed = lax.psum_scatter(
        jnp.dot(hidden, down_full, preferred_element_type=jnp.float32).astype(jnp.bfloat16),
        "tp",
        scatter_dimension=0,
        tiled=True,
    ).astype(jnp.float32)
    return (stream_f + 0.5 * summed).astype(jnp.bfloat16)


def local(
    stream,
    gain_first,
    gate_first,
    up_first,
    down_first,
    gain_second,
    gate_second,
    up_second,
    down_second,
):
    weights = gather_turned(
        (gate_first, up_first, down_first, gate_second, up_second, down_second),
        "fs",
        (0, 0, 1, 0, 0, 1),
    )
    first_set = (weights[0], weights[1], weights[2])
    second_set = (weights[3], weights[4], weights[5])
    middle = half_branch(stream, gain_first, first_set)
    return half_branch(middle, gain_second, second_set)


def solution(mesh):
    in_specs = (
        P(("grp", "fs", "tp"), None),
        P(),
        P("fs", "tp"),
        P("fs", "tp"),
        P("tp", "fs"),
        P(),
        P("fs", "tp"),
        P("fs", "tp"),
        P("tp", "fs"),
    )
    out_specs = P(("grp", "fs", "tp"), None)
    return jax.shard_map(local, mesh=mesh, in_specs=in_specs, out_specs=out_specs, check_vma=False)
```

profile of v0, /device:TPU:513, one launch (start us, length us, event | category | flops | bytes accessed | tf_op | source)
XLA Modules:
  0.0 377.2 jit_solution(9833353432578024981)
XLA Ops:
  6.6 1.3 fusion.18
  8.0 0.7 convert_element_type.43
  8.7 2.0 fusion.20
  10.8 0.1 all-gather.6.cloned.1.call-start
  10.9 0.1 copy.10
  11.0 0.1 copy.11
  11.2 0.1 copy.12
  11.3 0.1 copy.13
  11.6 0.9 copy-done.2
  12.5 0.1 reduce-scatter.3.cloned.1.call-start
  12.6 72.6 %all-gather.4.cloned.1.call-done = bf16[1024,2048]{1,0:T(8,128)(2,1)} async-done(((bf16[128,2048]{1,0:T(8,128)(2,1)}), bf16[1024,2048]{1,0:T(8,128)(2,1)}) %all-gather.4.cloned.1.call-update) | async-done | bytes 4194320 | tf_op jit(solution)/shard_map/all_gather | solution.py:28
  85.2 84.5 %all-gather.6.cloned.1.call-done = bf16[2048,3072]{0,1:T(8,128)(2,1)} async-done(((bf16[128,3072]{0,1:T(8,128)(2,1)}), bf16[2048,3072]{0,1:T(8,128)(2,1)}) %all-gather.6.cloned.1.call-update) | async-done | bytes 12582928 | tf_op jit(solution)/shard_map/all_gather | solution.py:11
  169.7 5.2 %fusion.8 = f32[1024,512]{1,0:T(8,128)S(1)} fusion(bf16[1024,2048]{1,0:T(8,128)(2,1)} %all-gather.4.cloned.1.call-done, bf16[2048,3072]{0,1:T(8,128)(2,1)} %all-gather.6.cloned.1.call-done), kind=kOutput, calls=%fused_computation.10 | convolution fusion | flops 2147483648 | bytes 8388608 | tf_op jit(solution)/shard_map/dot_general | solution.py:29
  174.9 10.0 %convolution_convert_fusion.1 = bf16[1024,2048]{1,0:T(8,128)(2,1)} fusion(bf16[2048,3072]{0,1:T(8,128)(2,1)} %all-gather.6.cloned.1.call-done, f32[1024,512]{1,0:T(8,128)S(1)} %fusion.8, bf16[1024,2048]{1,0:T(8,128)(2,1)} %all-gather.4.cloned.1.call-done), kind=kOutput, calls=%fused_computation.1 | convolution fusion | flops 4300210176 | bytes 14680064 | tf_op jit(solution)/shard_map/dot_general | solution.py:34
  185.1 0.5 copy-done.9
  185.6 53.6 %reduce-scatter.3.cloned.1.call-done = bf16[128,2048]{1,0:T(8,128)(2,1)} async-done(((bf16[1024,2048]{1,0:T(8,128)(2,1)}), bf16[128,2048]{1,0:T(8,128)(2,1)}) %reduce-scatter.3.cloned.1.call-update) | async-done | bytes 524304 | tf_op jit(solution)/shard_map/reduce_scatter | solution.py:33
  239.2 1.3 fusion.22
  240.6 2.1 fusion.24
  242.7 0.2 reduce-scatter.5.cloned.1.call-start
  243.0 54.6 %all-gather.8.cloned.1.call-done = bf16[1024,2048]{1,0:T(8,128)(2,1)} async-done(((bf16[128,2048]{1,0:T(8,128)(2,1)}), bf16[1024,2048]{1,0:T(8,128)(2,1)}) %all-gather.8.cloned.1.call-update) | async-done | bytes 4194320 | tf_op jit(solution)/shard_map/all_gather | solution.py:28
  297.6 5.2 %fusion.3 = f32[1024,512]{1,0:T(8,128)S(1)} fusion(bf16[1024,2048]{1,0:T(8,128)(2,1)} %all-gather.8.cloned.1.call-done, bf16[2048,3072]{0,1:T(8,128)(2,1)} %all-gather.6.cloned.1.call-done), kind=kOutput, calls=%fused_computation.5 | convolution fusion | flops 2147483648 | bytes 8388608 | tf_op jit(solution)/shard_map/dot_general | solution.py:29
  302.8 10.0 %convolution_convert_fusion = bf16[1024,2048]{1,0:T(8,128)(2,1)} fusion(bf16[2048,3072]{0,1:T(8,128)(2,1)} %all-gather.6.cloned.1.call-done, f32[1024,512]{1,0:T(8,128)S(1)} %fusion.3, bf16[1024,2048]{1,0:T(8,128)(2,1)} %all-gather.8.cloned.1.call-done), kind=kOutput, calls=%fused_computation | convolution fusion | flops 4300210176 | bytes 14680064 | tf_op jit(solution)/shard_map/dot_general | solution.py:34
  312.9 55.6 %reduce-scatter.5.cloned.1.call-done = bf16[128,2048]{1,0:T(8,128)(2,1)} async-done(((bf16[1024,2048]{1,0:T(8,128)(2,1)}), bf16[128,2048]{1,0:T(8,128)(2,1)}) %reduce-scatter.5.cloned.1.call-update) | async-done | bytes 524304 | tf_op jit(solution)/shard_map/reduce_scatter | solution.py:33
  368.5 2.1 fusion.25
  (34 shorter events, 0.6 us)
Async XLA Ops:
  6.5 4.3 %copy-start.3 = (bf16[128,512]{1,0:T(8,128)(2,1)S(1)}, bf16[128,512]{1,0:T(8,128)(2,1)}, u32[]{:S(2)}) copy-start(bf16[128,512]{1,0:T(8,128)(2,1)} %param.11) | copy-start | bytes 393220
  6.5 4.5 %copy-start.4 = (bf16[128,512]{1,0:T(8,128)(2,1)S(1)}, bf16[128,512]{1,0:T(8,128)(2,1)}, u32[]{:S(2)}) copy-start(bf16[128,512]{1,0:T(8,128)(2,1)} %param.12) | copy-start | bytes 393220
  6.6 4.6 %copy-start.5 = (bf16[128,512]{1,0:T(8,128)(2,1)S(1)}, bf16[128,512]{1,0:T(8,128)(2,1)}, u32[]{:S(2)}) copy-start(bf16[128,512]{1,0:T(8,128)(2,1)} %param.15) | copy-start | bytes 393220
  6.6 4.7 %copy-start.6 = (bf16[128,512]{1,0:T(8,128)(2,1)S(1)}, bf16[128,512]{1,0:T(8,128)(2,1)}, u32[]{:S(2)}) copy-start(bf16[128,512]{1,0:T(8,128)(2,1)} %param.16) | copy-start | bytes 393220
  6.6 4.9 %copy-start.7 = (bf16[512,128]{1,0:T(8,128)(2,1)S(1)}, bf16[512,128]{1,0:T(8,128)(2,1)}, u32[]{:S(2)}) copy-start(bf16[512,128]{1,0:T(8,128)(2,1)} %param.13) | copy-start | bytes 393220
  6.6 78.6 %all-gather.4.cloned.1.call-start = ((), (), s32[]{:S(2)}) async-start(), calls=%async_computation.2 | async-start | bytes 4718592 | tf_op jit(solution)/shard_map/all_gather | solution.py:28
  8.0 3.6 copy-start.8
  10.8 158.9 %all-gather.6.cloned.1.call-start = ((), (), s32[]{:S(2)}) async-start(), calls=%async_computation.3 | async-start | bytes 13369344 | tf_op jit(solution)/shard_map/all_gather | solution.py:11
  11.6 0.9 copy-start.2
  12.5 226.7 %reduce-scatter.3.cloned.1.call-start = ((), (), s32[]{:S(2)}) async-start(), calls=%async_computation.4 | async-start | bytes 4718592 | tf_op jit(solution)/shard_map/reduce_scatter | solution.py:33
  185.0 0.7 copy-start.9
  185.0 54.3 %copy-start = (bf16[128,2048]{1,0:T(8,128)(2,1)S(1)}, bf16[128,2048]{1,0:T(8,128)(2,1)}, u32[]{:S(2)}) copy-start(bf16[128,2048]{1,0:T(8,128)(2,1)} %param.9) | copy-start | bytes 1572868
  185.0 112.6 %all-gather.8.cloned.1.call-start = ((), (), s32[]{:S(2)}) async-start(), calls=%async_computation.5 | async-start | bytes 4718592 | tf_op jit(solution)/shard_map/all_gather | solution.py:28
  242.7 125.8 %reduce-scatter.5.cloned.1.call-start = ((), (), s32[]{:S(2)}) async-start(), calls=%async_computation.6 | async-start | bytes 4718592 | tf_op jit(solution)/shard_map/reduce_scatter | solution.py:33
  312.8 55.7 %copy-start.1 = (bf16[128,2048]{1,0:T(8,128)(2,1)S(1)}, bf16[128,2048]{1,0:T(8,128)(2,1)}, u32[]{:S(2)}) copy-start(bf16[128,2048]{1,0:T(8,128)(2,1)} %reduce-scatter.3.cloned.1.call-done) | copy-start | bytes 1572868
Sparse Core Ops, SparseCore 0:
  10.9 74.2 all-gather.3
  86.9 82.7 all-gather.5
  185.1 54.0 reduce-scatter.2
  242.8 54.7 all-gather.7
  313.0 55.4 reduce-scatter.4
where the time goes:
time: 377 us
  waiting for transfers between devices  321 us (85%)
  matrix products  30.5 us (8%)
  between operations  13.3 us (4%)
  other arithmetic  9.61 us (3%)
    all_gather x2, waiting for transfers between devices, half_branch(): tokens = lax.all_gather(normed, 'tp', axis=0, tiled=True)  127 us
    reduce_scatter x2, waiting for transfers between devices, half_branch(): lax.psum_scatter(jnp.dot(hidden, down_full, preferred_element_type=jnp.fl...  109 us
    all_gather x1, waiting for transfers between devices, gather_turned(): result = lax.all_gather(both, axis, axis=0, tiled=True)  84.5 us
    dot_general x2, matrix products, half_branch(): jnp.dot(hidden, down_full, preferred_element_type=jnp.float32)  20 us
    dot_general x2, matrix products, half_branch(): gate_act = jnp.dot(tokens, gathered[0], preferred_element_type=jnp.float32)  10.4 us
  transfers between devices with their start and end apart: 5, of which 5 were waited for; matrix products, arithmetic and copies ran while one was open for 0% of the time, Pallas kernels for 0%

commit v1 on v0

--- a/solution.py
+++ b/solution.py
@@ -25,7 +25,24 @@
         * lax.rsqrt(jnp.mean(stream_f * stream_f, axis=-1, keepdims=True) + 1e-06)
         * gain.astype(jnp.float32)
     ).astype(jnp.bfloat16)
-    tokens = lax.all_gather(normed, "tp", axis=0, tiled=True)
+    size, index, rows = (lax.axis_size("tp"), lax.axis_index("tp"), normed.shape[0])
+    forward = [(i, (i + 1) % size) for i in range(size)]
+    left = [(i, (i - 1) % size) for i in range(size)]
+    whole = jnp.zeros((*normed.shape[:0], size * rows, *normed.shape[0 + 1 :]), normed.dtype)
+    whole = lax.dynamic_update_slice_in_dim(whole, normed, index * rows, axis=0)
+    from_left = from_right = normed
+    middle_2 = size // 2
+    for step in range(1, middle_2 + 1):
+        from_left = lax.ppermute(from_left, "tp", forward)
+        whole = lax.dynamic_update_slice_in_dim(
+            whole, from_left, (index - step) % size * rows, axis=0
+        )
+        if step < size - middle_2:
+            from_right = lax.ppermute(from_right, "tp", left)
+            whole = lax.dynamic_update_slice_in_dim(
+                whole, from_right, (index + step) % size * rows, axis=0
+            )
+    tokens = whole
     gate_act = jnp.dot(tokens, gathered[0], preferred_element_type=jnp.float32)
     up_act = jnp.dot(tokens, gathered[1], preferred_element_type=jnp.float32)
     down_full = gathered[2]

time: 377 us -> 327 us (0.87)
  waiting for transfers between devices: 321 us -> 232 us
  starting transfers between devices: 0.5 us -> 21.7 us
  local copies, waits for them, and re-layouts: 2.05 us -> 18.7 us
    all_gather x2 -> x0, waiting for transfers between devices: 127 us -> none  [half_branch(): tokens = lax.all_gather(normed, 'tp', axis=0, tiled=True)]
    ppermute x0 -> x14, waiting for transfers between devices: none -> 73 us  [the longest x8 73 us: half_branch(): from_left = lax.ppermute(from_left, 'tp', forward)]
    all_gather x1, waiting for transfers between devices: 84.5 us -> 46.7 us  [gather_turned(): result = lax.all_gather(both, axis, axis=0, tiled=True)]
    ppermute x0 -> x14, starting transfers between devices: none -> 21.6 us  [the longest x6 16 us: half_branch(): from_right = lax.ppermute(from_right, 'tp', left)]
    unnamed x29 -> x19, local copies, waits for them, and re-layouts: 2.03 us -> 8.6 us
    dynamic_update_slice x0 -> x14, local copies, waits for them, and re-layouts: none -> 6.22 us  [the longest x8 3.54 us: half_branch(): lax.dynamic_update_slice_in_dim(whole, from_left, (index - step) % size *...]
    convert_element_type x2 -> x0, other arithmetic: 4.09 us -> none  [half_branch(): normed = (stream_f * lax.rsqrt(jnp.mean(stream_f * stream_f, axis=-1, kee...]
  transfers between devices with their start and end apart: 5 -> 17, of which waited for: 5 -> 11; matrix products, arithmetic and copies ran while one was open for 0% -> 4% of each run, Pallas kernels for 0% -> 0%
where the time goes in v1:
time: 327 us; the launch traced here: 326 us
  waiting for transfers between devices  232 us (71%)
  matrix products  33.3 us (10%)
  starting transfers between devices  21.7 us (7%)
  local copies, waits for them, and re-layouts  18.7 us (6%)
  between operations  13.3 us (4%)
  other arithmetic  6.7 us (2%)
    reduce_scatter x2, waiting for transfers between devices, half_branch(): lax.psum_scatter(jnp.dot(hidden, down_full, preferred_element_type=jnp.fl...  113 us
    ppermute x8, waiting for transfers between devices, half_branch(): from_left = lax.ppermute(from_left, 'tp', forward)  73 us
    all_gather x1, waiting for transfers between devices, gather_turned(): result = lax.all_gather(both, axis, axis=0, tiled=True)  46.7 us
    dot_general x2, matrix products, half_branch(): jnp.dot(hidden, down_full, preferred_element_type=jnp.float32)  21.4 us
    ppermute x6, starting transfers between devices, half_branch(): from_right = lax.ppermute(from_right, 'tp', left)  16 us
    dot_general x2, matrix products, half_branch(): up_act = jnp.dot(tokens, gathered[1], preferred_element_type=jnp.float32)  11.9 us
    unnamed x19, local copies, waits for them, and re-layouts  8.6 us
  transfers between devices with their start and end apart: 17, of which 11 were waited for; matrix products, arithmetic and copies ran while one was open for 4% of the time, Pallas kernels for 0%

profile of v1, /device:TPU:513, one launch (start us, length us, event | category | flops | bytes accessed | tf_op | source)
XLA Modules:
  0.0 326.3 jit_solution(5056681049691570151)
XLA Ops:
  15.7 2.5 broadcast.46.clone
  19.2 2.2 collective-permute-start
  21.3 2.2 collective-permute-start.1
  23.5 6.6 %collective-permute-done = bf16[128,2048]{1,0:T(8,128)(2,1)S(1)} collective-permute-done((bf16[128,2048]{1,0:T(8,128)(2,1)S(1)}, bf16[128,2048]{1,0:T(8,128)(2,1)S(1)}, u32[]{:S(2)}, u32[]{:S(2)}) %collective-permute-start) | collective-permute-done | bytes 524320 | tf_op jit(solution)/shard_map/ppermute | solution.py:36
  30.1 3.3 %collective-permute-start.2 = (bf16[128,2048]{1,0:T(8,128)(2,1)S(1)}, bf16[128,2048]{1,0:T(8,128)(2,1)S(1)}, u32[]{:S(2)}, u32[]{:S(2)}) collective-permute-start(bf16[128,2048]{1,0:T(8,128)(2,1)S(1)} %collective-permute-done), channel_id=1, source_target_pairs={{0,1},{1,2},{2,3},{3,4},{4,5},{5,6},{6,7},{7,0},{8,9},{9,10},{10,1... | collective-permute-start | bytes 1572872 | tf_op jit(solution)/shard_map/ppermute | solution.py:36
  33.4 3.0 collective-permute-start.3
  36.4 6.6 %collective-permute-done.2 = bf16[128,2048]{1,0:T(8,128)(2,1)S(1)} collective-permute-done((bf16[128,2048]{1,0:T(8,128)(2,1)S(1)}, bf16[128,2048]{1,0:T(8,128)(2,1)S(1)}, u32[]{:S(2)}, u32[]{:S(2)}) %collective-permute-start.2) | collective-permute-done | bytes 524320 | tf_op jit(solution)/shard_map/ppermute | solution.py:36
  44.7 2.7 collective-permute-start.5
  48.2 7.2 %collective-permute-done.4 = bf16[128,2048]{1,0:T(8,128)(2,1)S(1)} collective-permute-done((bf16[128,2048]{1,0:T(8,128)(2,1)S(1)}, bf16[128,2048]{1,0:T(8,128)(2,1)S(1)}, u32[]{:S(2)}, u32[]{:S(2)}) %collective-permute-start.4) | collective-permute-done | bytes 524320 | tf_op jit(solution)/shard_map/ppermute | solution.py:36
  57.9 10.5 %collective-permute-done.6 = bf16[128,2048]{1,0:T(8,128)(2,1)S(1)} collective-permute-done((bf16[128,2048]{1,0:T(8,128)(2,1)S(1)}, bf16[128,2048]{1,0:T(8,128)(2,1)S(1)}, u32[]{:S(2)}, u32[]{:S(2)}) %collective-permute-start.6) | collective-permute-done | bytes 524320 | tf_op jit(solution)/shard_map/ppermute | solution.py:36
  69.3 46.7 %all-gather.2.cloned.1.call-done = bf16[2048,3072]{0,1:T(8,128)(2,1)} async-done(((bf16[128,3072]{0,1:T(8,128)(2,1)}), bf16[2048,3072]{0,1:T(8,128)(2,1)}) %all-gather.2.cloned.1.call-update) | async-done | bytes 12582928 | tf_op jit(solution)/shard_map/all_gather | solution.py:11
  116.0 6.6 %fusion.6 = f32[1024,512]{1,0:T(8,128)} fusion(bf16[1024,2048]{1,0:T(8,128)(2,1)} %constant_dynamic-update-slice_fusion.12, bf16[2048,3072]{0,1:T(8,128)(2,1)} %all-gather.2.cloned.1.call-done), kind=kOutput, calls=%fused_computation.8 | convolution fusion | flops 2147483648 | bytes 8388608 | tf_op jit(solution)/shard_map/dot_general | solution.py:47
  122.6 10.7 %convolution_convert_fusion.1 = bf16[1024,2048]{1,0:T(8,128)(2,1)} fusion(bf16[2048,3072]{0,1:T(8,128)(2,1)} %all-gather.2.cloned.1.call-done, f32[1024,512]{1,0:T(8,128)} %fusion.6, bf16[1024,2048]{1,0:T(8,128)(2,1)} %constant_dynamic-update-slice_fusion.12), kind=kOutput, calls=%fused_computation.1 | convolution fusion | flops 4300210176 | bytes 14680064 | tf_op jit(solution)/shard_map/dot_general | solution.py:51
  134.0 53.6 %reduce-scatter.3.cloned.1.call-done = bf16[128,2048]{1,0:T(8,128)(2,1)} async-done(((bf16[1024,2048]{1,0:T(8,128)(2,1)}), bf16[128,2048]{1,0:T(8,128)(2,1)}) %reduce-scatter.3.cloned.1.call-update) | async-done | bytes 524304 | tf_op jit(solution)/shard_map/reduce_scatter | solution.py:50
  189.9 2.6 collective-permute-start.8
  192.6 11.3 %collective-permute-done.7 = bf16[128,2048]{1,0:T(8,128)(2,1)S(1)} collective-permute-done((bf16[128,2048]{1,0:T(8,128)(2,1)S(1)}, bf16[128,2048]{1,0:T(8,128)(2,1)S(1)}, u32[]{:S(2)}, u32[]{:S(2)}) %collective-permute-start.7) | collective-permute-done | bytes 524320 | tf_op jit(solution)/shard_map/ppermute | solution.py:36
  203.8 2.7 collective-permute-start.10
  206.5 10.4 %collective-permute-done.9 = bf16[128,2048]{1,0:T(8,128)(2,1)S(1)} collective-permute-done((bf16[128,2048]{1,0:T(8,128)(2,1)S(1)}, bf16[128,2048]{1,0:T(8,128)(2,1)S(1)}, u32[]{:S(2)}, u32[]{:S(2)}) %collective-permute-start.9) | collective-permute-done | bytes 524320 | tf_op jit(solution)/shard_map/ppermute | solution.py:36
  217.1 2.8 collective-permute-start.12
  219.9 9.3 %collective-permute-done.11 = bf16[128,2048]{1,0:T(8,128)(2,1)S(1)} collective-permute-done((bf16[128,2048]{1,0:T(8,128)(2,1)S(1)}, bf16[128,2048]{1,0:T(8,128)(2,1)S(1)}, u32[]{:S(2)}, u32[]{:S(2)}) %collective-permute-start.11) | collective-permute-done | bytes 524320 | tf_op jit(solution)/shard_map/ppermute | solution.py:36
  229.4 11.2 %collective-permute-done.13 = bf16[128,2048]{1,0:T(8,128)(2,1)S(1)} collective-permute-done((bf16[128,2048]{1,0:T(8,128)(2,1)S(1)}, bf16[128,2048]{1,0:T(8,128)(2,1)S(1)}, u32[]{:S(2)}, u32[]{:S(2)}) %collective-permute-start.13) | collective-permute-done | bytes 524320 | tf_op jit(solution)/shard_map/ppermute | solution.py:36
  242.6 5.3 %fusion.1 = f32[1024,512]{1,0:T(8,128)} fusion(bf16[1024,2048]{1,0:T(8,128)(2,1)S(1)} %constant_dynamic-update-slice_fusion.4, bf16[2048,3072]{0,1:T(8,128)(2,1)} %all-gather.2.cloned.1.call-done), kind=kOutput, calls=%fused_computation.3 | convolution fusion | flops 2147483648 | bytes 8388608 | tf_op jit(solution)/shard_map/dot_general | solution.py:47
  247.9 10.7 %convolution_convert_fusion = bf16[1024,2048]{1,0:T(8,128)(2,1)} fusion(bf16[2048,3072]{0,1:T(8,128)(2,1)} %all-gather.2.cloned.1.call-done, f32[1024,512]{1,0:T(8,128)} %fusion.1, bf16[1024,2048]{1,0:T(8,128)(2,1)} %copy-done.2), kind=kOutput, calls=%fused_computation | convolution fusion | flops 4300210176 | bytes 14680064 | tf_op jit(solution)/shard_map/dot_general | solution.py:51
  258.6 59.0 %reduce-scatter.5.cloned.1.call-done = bf16[128,2048]{1,0:T(8,128)(2,1)} async-done(((bf16[1024,2048]{1,0:T(8,128)(2,1)}), bf16[128,2048]{1,0:T(8,128)(2,1)}) %reduce-scatter.5.cloned.1.call-update) | async-done | bytes 524304 | tf_op jit(solution)/shard_map/reduce_scatter | solution.py:50
  (62 shorter events, 23.4 us)
Async XLA Ops:
  6.5 11.6 %copy-start = (bf16[128,2048]{1,0:T(8,128)(2,1)S(1)}, bf16[128,2048]{1,0:T(8,128)(2,1)}, u32[]{:S(2)}) copy-start(bf16[128,2048]{1,0:T(8,128)(2,1)} %param.9) | copy-start | bytes 1572868
  6.5 109.4 %all-gather.2.cloned.1.call-start = ((), (), s32[]{:S(2)}) async-start(), calls=%async_computation.2 | async-start | bytes 13369344 | tf_op jit(solution)/shard_map/all_gather | solution.py:11
  12.7 1.0 copy-start.3
  13.7 173.8 %reduce-scatter.3.cloned.1.call-start = ((), (), s32[]{:S(2)}) async-start(), calls=%async_computation.3 | async-start | bytes 4718592 | tf_op jit(solution)/shard_map/reduce_scatter | solution.py:50
  19.2 10.9 %collective-permute-start = (bf16[128,2048]{1,0:T(8,128)(2,1)S(1)}, bf16[128,2048]{1,0:T(8,128)(2,1)S(1)}, u32[]{:S(2)}, u32[]{:S(2)}) collective-permute-start(bf16[128,2048]{1,0:T(8,128)(2,1)S(1)} %get-tuple-element.8), channel_id=1, source_target_pairs={{0,1},{1,2},{2,3},{3,4},{4,5},{5,6},{6,7},{7,0},{8,9},{9,10},{10,1... | collective-permute-start | bytes 1572872 | tf_op jit(solution)/shard_map/ppermute | solution.py:36
  21.3 12.0 %collective-permute-start.1 = (bf16[128,2048]{1,0:T(8,128)(2,1)S(1)}, bf16[128,2048]{1,0:T(8,128)(2,1)S(1)}, u32[]{:S(2)}, u32[]{:S(2)}) collective-permute-start(bf16[128,2048]{1,0:T(8,128)(2,1)S(1)} %get-tuple-element.8), channel_id=1, source_target_pairs={{0,7},{1,0},{2,1},{3,2},{4,3},{5,4},{6,5},{7,6},{8,15},{9,8},{10,9... | collective-permute-start | bytes 1572872 | tf_op jit(solution)/shard_map/ppermute | solution.py:41
  30.1 12.9 %collective-permute-start.2 = (bf16[128,2048]{1,0:T(8,128)(2,1)S(1)}, bf16[128,2048]{1,0:T(8,128)(2,1)S(1)}, u32[]{:S(2)}, u32[]{:S(2)}) collective-permute-start(bf16[128,2048]{1,0:T(8,128)(2,1)S(1)} %collective-permute-done), channel_id=1, source_target_pairs={{0,1},{1,2},{2,3},{3,4},{4,5},{5,6},{6,7},{7,0},{8,9},{9,10},{10,1... | collective-permute-start | bytes 1572872 | tf_op jit(solution)/shard_map/ppermute | solution.py:36
  33.4 11.3 %collective-permute-start.3 = (bf16[128,2048]{1,0:T(8,128)(2,1)S(1)}, bf16[128,2048]{1,0:T(8,128)(2,1)S(1)}, u32[]{:S(2)}, u32[]{:S(2)}) collective-permute-start(bf16[128,2048]{1,0:T(8,128)(2,1)S(1)} %collective-permute-done.1), channel_id=1, source_target_pairs={{0,7},{1,0},{2,1},{3,2},{4,3},{5,4},{6,5},{7,6},{8,15},{9,8},{10,9... | collective-permute-start | bytes 1572872 | tf_op jit(solution)/shard_map/ppermute | solution.py:41
  43.0 12.3 %collective-permute-start.4 = (bf16[128,2048]{1,0:T(8,128)(2,1)S(1)}, bf16[128,2048]{1,0:T(8,128)(2,1)S(1)}, u32[]{:S(2)}, u32[]{:S(2)}) collective-permute-start(bf16[128,2048]{1,0:T(8,128)(2,1)S(1)} %collective-permute-done.2), channel_id=1, source_target_pairs={{0,1},{1,2},{2,3},{3,4},{4,5},{5,6},{6,7},{7,0},{8,9},{9,10},{10,1... | collective-permute-start | bytes 1572872 | tf_op jit(solution)/shard_map/ppermute | solution.py:36
  44.7 12.4 %collective-permute-start.5 = (bf16[128,2048]{1,0:T(8,128)(2,1)S(1)}, bf16[128,2048]{1,0:T(8,128)(2,1)S(1)}, u32[]{:S(2)}, u32[]{:S(2)}) collective-permute-start(bf16[128,2048]{1,0:T(8,128)(2,1)S(1)} %collective-permute-done.3), channel_id=1, source_target_pairs={{0,7},{1,0},{2,1},{3,2},{4,3},{5,4},{6,5},{7,6},{8,15},{9,8},{10,9... | collective-permute-start | bytes 1572872 | tf_op jit(solution)/shard_map/ppermute | solution.py:41
  55.3 13.1 %collective-permute-start.6 = (bf16[128,2048]{1,0:T(8,128)(2,1)S(1)}, bf16[128,2048]{1,0:T(8,128)(2,1)S(1)}, u32[]{:S(2)}, u32[]{:S(2)}) collective-permute-start(bf16[128,2048]{1,0:T(8,128)(2,1)S(1)} %collective-permute-done.4), channel_id=1, source_target_pairs={{0,1},{1,2},{2,3},{3,4},{4,5},{5,6},{6,7},{7,0},{8,9},{9,10},{10,1... | collective-permute-start | bytes 1572872 | tf_op jit(solution)/shard_map/ppermute | solution.py:36
  133.3 0.7 copy-start.4
  133.3 184.3 %reduce-scatter.5.cloned.1.call-start = ((), (), s32[]{:S(2)}) async-start(), calls=%async_computation.4 | async-start | bytes 4718592 | tf_op jit(solution)/shard_map/reduce_scatter | solution.py:50
  187.5 1.9 copy-start.1
  189.8 14.1 %collective-permute-start.7 = (bf16[128,2048]{1,0:T(8,128)(2,1)S(1)}, bf16[128,2048]{1,0:T(8,128)(2,1)S(1)}, u32[]{:S(2)}, u32[]{:S(2)}) collective-permute-start(bf16[128,2048]{1,0:T(8,128)(2,1)S(1)} %get-tuple-element.6), channel_id=1, source_target_pairs={{0,1},{1,2},{2,3},{3,4},{4,5},{5,6},{6,7},{7,0},{8,9},{9,10},{10,1... | collective-permute-start | bytes 1572872 | tf_op jit(solution)/shard_map/ppermute | solution.py:36
  189.9 13.9 %collective-permute-start.8 = (bf16[128,2048]{1,0:T(8,128)(2,1)S(1)}, bf16[128,2048]{1,0:T(8,128)(2,1)S(1)}, u32[]{:S(2)}, u32[]{:S(2)}) collective-permute-start(bf16[128,2048]{1,0:T(8,128)(2,1)S(1)} %get-tuple-element.6), channel_id=1, source_target_pairs={{0,7},{1,0},{2,1},{3,2},{4,3},{5,4},{6,5},{7,6},{8,15},{9,8},{10,9... | collective-permute-start | bytes 1572872 | tf_op jit(solution)/shard_map/ppermute | solution.py:41
  203.8 13.1 %collective-permute-start.9 = (bf16[128,2048]{1,0:T(8,128)(2,1)S(1)}, bf16[128,2048]{1,0:T(8,128)(2,1)S(1)}, u32[]{:S(2)}, u32[]{:S(2)}) collective-permute-start(bf16[128,2048]{1,0:T(8,128)(2,1)S(1)} %collective-permute-done.7), channel_id=1, source_target_pairs={{0,1},{1,2},{2,3},{3,4},{4,5},{5,6},{6,7},{7,0},{8,9},{9,10},{10,1... | collective-permute-start | bytes 1572872 | tf_op jit(solution)/shard_map/ppermute | solution.py:36
  203.8 13.2 %collective-permute-start.10 = (bf16[128,2048]{1,0:T(8,128)(2,1)S(1)}, bf16[128,2048]{1,0:T(8,128)(2,1)S(1)}, u32[]{:S(2)}, u32[]{:S(2)}) collective-permute-start(bf16[128,2048]{1,0:T(8,128)(2,1)S(1)} %collective-permute-done.8), channel_id=1, source_target_pairs={{0,7},{1,0},{2,1},{3,2},{4,3},{5,4},{6,5},{7,6},{8,15},{9,8},{10,9... | collective-permute-start | bytes 1572872 | tf_op jit(solution)/shard_map/ppermute | solution.py:41
  216.9 12.2 %collective-permute-start.11 = (bf16[128,2048]{1,0:T(8,128)(2,1)S(1)}, bf16[128,2048]{1,0:T(8,128)(2,1)S(1)}, u32[]{:S(2)}, u32[]{:S(2)}) collective-permute-start(bf16[128,2048]{1,0:T(8,128)(2,1)S(1)} %collective-permute-done.9), channel_id=1, source_target_pairs={{0,1},{1,2},{2,3},{3,4},{4,5},{5,6},{6,7},{7,0},{8,9},{9,10},{10,1... | collective-permute-start | bytes 1572872 | tf_op jit(solution)/shard_map/ppermute | solution.py:36
  217.1 12.2 %collective-permute-start.12 = (bf16[128,2048]{1,0:T(8,128)(2,1)S(1)}, bf16[128,2048]{1,0:T(8,128)(2,1)S(1)}, u32[]{:S(2)}, u32[]{:S(2)}) collective-permute-start(bf16[128,2048]{1,0:T(8,128)(2,1)S(1)} %collective-permute-done.10), channel_id=1, source_target_pairs={{0,7},{1,0},{2,1},{3,2},{4,3},{5,4},{6,5},{7,6},{8,15},{9,8},{10,9... | collective-permute-start | bytes 1572872 | tf_op jit(solution)/shard_map/ppermute | solution.py:41
  229.2 11.4 %collective-permute-start.13 = (bf16[128,2048]{1,0:T(8,128)(2,1)S(1)}, bf16[128,2048]{1,0:T(8,128)(2,1)S(1)}, u32[]{:S(2)}, u32[]{:S(2)}) collective-permute-start(bf16[128,2048]{1,0:T(8,128)(2,1)S(1)} %collective-permute-done.11), channel_id=1, source_target_pairs={{0,1},{1,2},{2,3},{3,4},{4,5},{5,6},{6,7},{7,0},{8,9},{9,10},{10,1... | collective-permute-start | bytes 1572872 | tf_op jit(solution)/shard_map/ppermute | solution.py:36
  240.6 2.0 copy-start.2
Sparse Core Ops, SparseCore 0:
  13.8 102.1 all-gather.1
  133.5 54.0 reduce-scatter.2
  258.7 58.8 reduce-scatter.4
